TPU v7x, 128 devices: a whole 4x4x4 slice. The times are simulated.
128 devices in a mesh: dp: 4 (over x), kv: 16 (over z, y), tp: 2 (over core).
Axes of the slice: x: 4, y: 4, z: 4, core: 2. Of those that a mesh axis runs over, the one named last changes fastest.
Arguments:
- tokens: bfloat16 [32, 2048], P('dp', ('kv', 'tp')), may hold values from -30 to 30
- attention_gain: bfloat16 [2048], P(('kv', 'tp')), may hold values from 0.099609375 to 1.8984375
- query_one: bfloat16 [2048, 512], P('kv', 'tp'), may hold values from -0.125 to 0.125
- query_two: bfloat16 [2048, 512], P('kv', 'tp'), may hold values from -0.125 to 0.125
- key_one: bfloat16 [2048, 512], P('kv', 'tp'), may hold values from -2 to 2
- key_two: bfloat16 [2048, 512], P('kv', 'tp'), may hold values from -2 to 2
- value_weight: bfloat16 [2048, 1024], P('kv', 'tp'), may hold values from -0.125 to 0.125
- head_second_weight: float32 [8], P('tp'), may hold values from 0.3 to 0.8
- head_gain: float32 [128], replicated, may hold values from 0.1 to 1.9
- out_weight: bfloat16 [1024, 2048], P('tp', 'kv'), may hold values from -0.375 to 0.375
- mixer_gain: bfloat16 [2048], P(('kv', 'tp')), may hold values from 0.099609375 to 1.8984375
- gate_weight: bfloat16 [2048, 5632], P('kv', 'tp'), may hold values from -0.125 to 0.125
- up_weight: bfloat16 [2048, 5632], P('kv', 'tp'), may hold values from -0.125 to 0.125
- down_weight: bfloat16 [5632, 2048], P('tp', 'kv'), may hold values from -0.15625 to 0.15625
- key_cache: bfloat16 [32, 16384, 8, 128], P('dp', 'kv', 'tp'), may hold values from -240 to 240
- value_cache: bfloat16 [32, 16384, 8, 128], P('dp', 'kv', 'tp'), may hold values from -6 to 6
Outputs:
- layer_out: bfloat16 [32, 2048], P('dp', ('kv', 'tp'))
All inputs are finite; a program needn't handle non-finite values.
Results may differ from a plain program's by a relative error of at most 0.02.
Values may be sent and summed in bfloat16 or wider, within the bound.
A program may use at most 64 MiB of HBM per device.

v0:
```python
import jax
import jax.numpy as jnp
from jax import lax
from jax.sharding import Mesh
from jax.sharding import PartitionSpec as P

DH = 64
KV = ("kv_0", "kv_1")
KV_TP = ("kv_0", "kv_1", "tp")
NORM_EPSILON = 1e-06
HEAD_EPSILON = 1e-05
HEAD_SCALE = 0.8
ROTARY_BASE = 10000.0


def turned_gather(arrays, axis, dims):
    turned = [jnp.moveaxis(a, dim, 0) for a, dim in zip(arrays, dims)]
    both = jnp.concatenate([t.reshape(len(t), -1) for t in turned], axis=1)
    filled, at, done = (lax.all_gather(both, axis, axis=0, tiled=True), 0, [])
    for t, dim in zip(turned, dims):
        piece = filled[:, at : at + t[0].size].reshape(-1, *t.shape[1:])
        done.append(jnp.moveaxis(piece, 0, dim))
        at += t[0].size
    return tuple(done)


def copy_for_each(value, axis):
    copies = jnp.broadcast_to(value, (lax.axis_size(axis), *value.shape))
    return lax.all_to_all(copies, axis, split_axis=0, concat_axis=0, tiled=True)


def of_everyone(value, axis):
    everything = copy_for_each(value, axis)
    return jnp.sum(everything, axis=0)


def in_one(arrays, axis):
    line, at, done = (jnp.concatenate([a.reshape(-1) for a in arrays]), 0, [])
    subtotal = of_everyone(line, axis)
    for a in arrays:
        done.append(subtotal[at : at + a.size].reshape(a.shape))
        at += a.size
    return tuple(done)


def collected_together(value, axis):
    leaves = jax.tree.leaves(value)
    turns = sorted(range(len(leaves)), key=lambda k: -leaves[k].size)
    width = (1, *leaves[turns[0]].shape)[-1]
    lines = [
        jnp.pad(leaves[k].reshape(-1), (0, -leaves[k].size % width)).reshape(-1, width)
        for k in turns
    ]
    both, at, found = (lax.all_gather(jnp.concatenate(lines), axis), 0, {})
    for k, line in zip(turns, lines):
        piece = both[:, at : at + len(line)].reshape(len(both), -1)
        found[k] = piece[:, : leaves[k].size].reshape(-1, *leaves[k].shape)
        at += len(line)
    numbers = iter(range(len(leaves)))
    return jax.tree.map(lambda _: found[next(numbers)], value)


def joined_all(value, axes, combine):
    for axis in axes:
        pieces = collected_together(value, axis)
        value = jax.tree.map(lambda part: part[0], pieces)
        for k in range(1, lax.axis_size(axis)):
            value = combine(value, jax.tree.map(lambda part: part[k], pieces))
    return value


def split_up(value, dim, devices):
    before, after = (value.shape[:dim], value.shape[dim + 1 :])
    return jnp.moveaxis(value.reshape(*before, devices, -1, *after), dim, 0)


def sent_and_summed(value, axis, dim):
    parts = split_up(value, dim, lax.axis_size(axis))
    arrived = lax.all_to_all(parts, axis, split_axis=0, concat_axis=0, tiled=True)
    return arrived.astype(jnp.float32).sum(axis=0)


def sent_and_summed_2(value, axis, dim):
    devices = lax.axis_size(axis)
    parts = lax.all_to_all(split_up(value, dim, devices), axis, 0, 0, tiled=True)
    return jnp.sum(parts, axis=0)


def in_one_piece(arrays, axis, dim, along):
    both = jnp.concatenate(arrays, axis=along)
    filled, at, done = (sent_and_summed_2(both, axis, dim), 0, [])
    for a in arrays:
        done.append(lax.slice_in_dim(filled, at, at + a.shape[along], axis=along))
        at += a.shape[along]
    return tuple(done)


def laid_out(parts, dim):
    shape = list(parts.shape[1:])
    shape[dim] *= parts.shape[0]
    return jnp.moveaxis(parts, 0, dim).reshape(shape)


def gathered_copies(value, axis, dim):
    parts = copy_for_each(value, axis)
    return laid_out(parts, dim)


def rotate(vectors, position):
    half_width = vectors.shape[-1] // 2
    frequency = 1.0 / ROTARY_BASE ** (jnp.arange(half_width, dtype=jnp.float32) / half_width)
    angles = position * frequency
    cosine = jnp.cos(angles)
    sine_value = jnp.sin(angles)
    lead_half = vectors[..., :half_width]
    tail_half = vectors[..., half_width:]
    return jnp.concatenate(
        [lead_half * cosine - tail_half * sine_value, tail_half * cosine + lead_half * sine_value],
        axis=-1,
    )


def combine(earlier, later):
    peak_left, total_left, weighted_left = earlier
    peak_right, total_right, weighted_right = later
    peak_score = jnp.maximum(peak_left, peak_right)
    factor_left = jnp.exp(peak_left - peak_score)
    factor_right = jnp.exp(peak_right - peak_score)
    return (
        peak_score,
        total_left * factor_left + total_right * factor_right,
        weighted_left * factor_left[..., None] + weighted_right * factor_right[..., None],
    )


def shards(
    tokens,
    attention_gain,
    query_one,
    query_two,
    key_one,
    key_two,
    value_weight,
    head_second_weight,
    head_gain,
    out_weight,
    mixer_gain,
    gate_weight,
    up_weight,
    down_weight,
    key_cache,
    value_cache,
):
    row_count = tokens.shape[0]
    position_group = lax.axis_size(KV)
    model_width = tokens.shape[1] * position_group * lax.axis_size("tp")
    local_heads = query_one.shape[1] // DH
    local_positions = key_cache.shape[1]
    position = jnp.float32(local_positions * position_group)
    score_scale = DH ** (-0.5)
    token_values = tokens.astype(jnp.float32)
    row_block, gain_block = turned_gather((tokens, attention_gain), "tp", (1, 0))
    block_values = row_block.astype(jnp.float32)
    scaled = (block_values * gain_block.astype(jnp.float32)).astype(jnp.bfloat16)
    query_first = jnp.dot(scaled, query_one, preferred_element_type=jnp.float32)
    query_second = jnp.dot(scaled, query_two, preferred_element_type=jnp.float32)
    key_first = jnp.dot(scaled, key_one, preferred_element_type=jnp.float32)
    key_second = jnp.dot(scaled, key_two, preferred_element_type=jnp.float32)
    value_part = jnp.dot(scaled, value_weight, preferred_element_type=jnp.float32)
    block_square = jnp.sum(block_values * block_values, axis=1)
    query_first, query_second, key_first, key_second, value_part, square_total = in_one(
        (query_first, query_second, key_first, key_second, value_part, block_square), KV
    )
    row_ratio = lax.rsqrt(square_total / model_width + NORM_EPSILON)[:, None]

    def paired(lead_part, tail_part):
        both = jnp.stack(
            [
                (lead_part * row_ratio).reshape(row_count, local_heads, DH),
                (tail_part * row_ratio).reshape(row_count, local_heads, DH),
            ],
            axis=2,
        )
        return rotate(both, position).astype(jnp.bfloat16)

    queries = paired(query_first, query_second)
    new_keys = paired(key_first, key_second)
    new_values = (
        (value_part * row_ratio).astype(jnp.bfloat16).reshape(row_count, local_heads, 2 * DH)
    )
    zero_half = jnp.zeros((row_count, local_heads, DH), jnp.bfloat16)
    padded_query_rows = jnp.stack(
        [
            jnp.concatenate([queries[:, :, 0], zero_half], axis=-1),
            jnp.concatenate([zero_half, queries[:, :, 1]], axis=-1),
        ],
        axis=2,
    )
    logit_scores = (
        jnp.einsum(
            "bhmk,bphk->bhmp", padded_query_rows, key_cache, preferred_element_type=jnp.float32
        )
        * score_scale
    )
    peak_score = jnp.max(logit_scores, axis=-1)
    exponent = jnp.exp(logit_scores - peak_score[..., None])
    weight_sum = jnp.sum(exponent, axis=-1)
    weighted = jnp.einsum(
        "bhmp,bphe->bhme",
        exponent.astype(jnp.bfloat16),
        value_cache,
        preferred_element_type=jnp.float32,
    )
    peak_score, weight_sum, weighted = joined_all((peak_score, weight_sum, weighted), KV, combine)
    own_score = (
        jnp.sum(queries.astype(jnp.float32) * new_keys.astype(jnp.float32), axis=-1) * score_scale
    )
    final_peak = jnp.maximum(peak_score, own_score)
    cache_factor = jnp.exp(peak_score - final_peak)
    own_weight = jnp.exp(own_score - final_peak)
    weight_sum = weight_sum * cache_factor + own_weight
    weighted = (
        weighted * cache_factor[..., None]
        + own_weight[..., None] * new_values.astype(jnp.float32)[:, :, None, :]
    )
    averaged = weighted / weight_sum[..., None]
    difference = averaged[:, :, 0] - head_second_weight[None, :, None] * averaged[:, :, 1]
    inverse_norm = lax.rsqrt(
        jnp.mean(difference * difference, axis=-1, keepdims=True) + HEAD_EPSILON
    )
    attended = (difference * inverse_norm * head_gain[None, None, :] * HEAD_SCALE).astype(
        jnp.bfloat16
    )
    attended = attended.reshape(row_count, local_heads * 2 * DH)
    attention_term = jnp.dot(attended, out_weight, preferred_element_type=jnp.float32)
    attention_out = sent_and_summed(attention_term.astype(jnp.bfloat16), "tp", 1)
    mixed = (token_values + attention_out).astype(jnp.bfloat16)
    mixed_values = mixed.astype(jnp.float32)
    mixer_block, mixer_gain_block = turned_gather((mixed, mixer_gain), "tp", (1, 0))
    mixer_block_values = mixer_block.astype(jnp.float32)
    mixer_scaled = (mixer_block_values * mixer_gain_block.astype(jnp.float32)).astype(jnp.bfloat16)
    gate_part = jnp.dot(mixer_scaled, gate_weight, preferred_element_type=jnp.float32)
    up_part = jnp.dot(mixer_scaled, up_weight, preferred_element_type=jnp.float32)
    mixer_square = jnp.sum(mixer_block_values * mixer_block_values, axis=1)
    square_columns = jnp.broadcast_to(mixer_square[:, None], (row_count, position_group))
    gate_sum, up_sum, total_column = (
        *in_one_piece((gate_part, up_part), KV, 1, 0),
        sent_and_summed_2(square_columns, KV, 1),
    )
    mixer_total = total_column[:, 0]
    mixer_ratio = lax.rsqrt(mixer_total / model_width + NORM_EPSILON)[:, None]
    hidden_share = (jax.nn.silu(gate_sum * mixer_ratio) * (up_sum * mixer_ratio)).astype(
        jnp.bfloat16
    )
    hidden_state = gathered_copies(hidden_share, KV, 1)
    mixer_term = jnp.dot(hidden_state, down_weight, preferred_element_type=jnp.float32)
    mixer_out = sent_and_summed(mixer_term.astype(jnp.bfloat16), "tp", 1)
    return (mixed_values + mixer_out).astype(jnp.bfloat16)


def solution(mesh):
    torus = Mesh(
        mesh.devices.reshape(mesh.shape["dp"], 4, 4, mesh.shape["tp"]), ("dp", "kv_0", "kv_1", "tp")
    )
    return jax.shard_map(
        shards,
        mesh=torus,
        in_specs=(
            P("dp", KV_TP),
            P(KV_TP),
            P(KV, "tp"),
            P(KV, "tp"),
            P(KV, "tp"),
            P(KV, "tp"),
            P(KV, "tp"),
            P("tp"),
            P(),
            P("tp", KV),
            P(KV_TP),
            P(KV, "tp"),
            P(KV, "tp"),
            P("tp", KV),
            P("dp", KV, "tp", None),
            P("dp", KV, "tp", None),
        ),
        out_specs=P("dp", KV_TP),
        check_vma=False,
    )
```

profile of v0, /device:TPU:1, one launch (start us, length us, event | category | flops | bytes accessed | tf_op | source)
XLA Modules:
  0.0 119.3 jit_solution(6227983753720261710)
XLA Ops:
  0.0 0.8 maximum_bitcast_fusion.2
  0.8 2.8 %all-gather.2 = bf16[2,64,9]{1,2,0:T(8,128)(2,1)S(1)} all-gather(bf16[1,64,9]{1,2,0:T(8,128)(2,1)S(1)} %maximum_bitcast_fusion.2), channel_id=1, replica_groups=mesh['dp'=4,'kv_0'=4,'kv_1'=4,'tp'=2] {'tp'}, dimensions={0}, use_global_device_ids=true | all-gather | bytes 3456 | tf_op jit(solution)/shard_map/all_gather | solution.py:19
  3.8 1.0 convolution_bitcast_fusion.4
  4.8 1.0 convolution_bitcast_fusion.3
  5.8 1.0 convolution_bitcast_fusion.2
  6.8 1.0 convolution_bitcast_fusion.1
  7.8 1.0 convolution_bitcast_fusion
  8.8 1.3 %broadcast_in_dim.4 = f32[16,1,12296]{2,1,0:T(1,128)} broadcast(f32[12296]{0:T(1024)S(1)} %constant_dynamic-update-slice_fusion), dimensions={2} | broadcast | bytes 836128 | tf_op jit(solution)/shard_map/broadcast_in_dim | solution.py:28
  10.1 7.9 %all-to-all-start = ((f32[16,1,12296]{2,1,0:T(1,128)}), f32[16,1,12296]{2,1,0:T(1,128)S(1)}, u32[]{:S(2)}, u32[]{:S(2)}) async-start(f32[16,1,12296]{2,1,0:T(1,128)} %broadcast_in_dim.4), calls=%async_computation | async-start | bytes 1589248 | tf_op jit(solution)/shard_map/all_to_all | solution.py:29
  18.1 0.7 broadcast_bitcast_fusion
  18.8 12.8 %all-to-all-done = f32[16,1,12296]{2,1,0:T(1,128)S(1)} async-done(((f32[16,1,12296]{2,1,0:T(1,128)}), f32[16,1,12296]{2,1,0:T(1,128)S(1)}, u32[]{:S(2)}, u32[]{:S(2)}) %all-to-all-start) | async-done | bytes 786976 | tf_op jit(solution)/shard_map/all_to_all | solution.py:29
  31.7 0.5 reduce_sum.91
  32.9 5.7 %fusion.94 = (f32[8,4,2]{2,1,0:T(4,128)S(1)}, f32[8,4,2,1024]{3,2,1,0:T(2,128)S(1)}) fusion(bf16[8,1024,4,128]{3,2,1,0:T(4,128)(2,1)} %param.30, bf16[8,4,1,128]{3,2,1,0:T(2,128)(2,1)S(1)} %copy.107, bf16[8,4,1,128]{3,2,1,0:T(2,128)(2,1)S(1)} %copy.106), kind=kOutput, calls=%fused_computation.184 | convolution fusion | flops 16940992 | bytes 8667392 | tf_op jit(solution)/shard_map/bhmk,bphk->bhmp/dot_general | solution.py:200
  38.7 0.1 reshape.556
  38.8 0.3 fusion.7
  39.2 4.9 %fusion = f32[8,4,2,128]{3,2,1,0:T(2,128)S(1)} fusion(bf16[8,1024,4,128]{3,2,1,0:T(4,128)(2,1)} %param.31, f32[8,4,2,1024]{3,2,1,0:T(2,128)S(1)} %get-tuple-element.57, f32[8,4,2]{2,1,0:T(4,128)S(1)} %get-tuple-element.56), kind=kOutput, calls=%fused_computation | convolution fusion | flops 16908288 | bytes 8683776 | tf_op jit(solution)/shard_map/bhmp,bphe->bhme/dot_general | solution.py:208
  44.3 9.6 %all-gather.3 = f32[4,66,128]{2,1,0:T(8,128)S(1)} all-gather(f32[1,66,128]{2,1,0:T(8,128)S(1)} %maximum_bitcast_fusion), channel_id=2, replica_groups=mesh['dp'=4,'kv_0'=4,'kv_1'=4,'tp'=2] {'kv_0'}, dimensions={0}, use_global_device_ids=true | all-gather | bytes 168960 | tf_op jit(solution)/shard_map/all_gather | solution.py:54
  54.0 9.6 %all-gather.4 = f32[4,66,128]{2,1,0:T(8,128)S(1)} all-gather(f32[1,66,128]{2,1,0:T(8,128)S(1)} %maximum_bitcast_fusion.1), channel_id=3, replica_groups=mesh['dp'=4,'kv_0'=4,'kv_1'=4,'tp'=2] {'kv_1'}, dimensions={0}, use_global_device_ids=true | all-gather | bytes 168960 | tf_op jit(solution)/shard_map/all_gather | solution.py:54
  63.8 0.1 copy.111
  64.1 0.1 copy.112
  64.3 0.1 copy.116
  64.5 0.1 squeeze.109
  64.6 0.1 copy.119
  64.9 0.1 copy.122
  65.2 0.1 copy.123
  65.3 0.1 squeeze.113
  65.4 0.1 copy.124
  65.7 0.1 copy.125
  65.9 0.2 multiply_reduce_fusion
  66.1 0.2 fusion.23
  66.4 0.2 fusion.38
  66.6 0.2 convolution_convert_fusion.1
  67.0 10.2 %all_to_all.31 = bf16[2,2,256]{2,1,0:T(2,128)(2,1)S(1)} all-to-all(bf16[2,2,256]{2,1,0:T(2,128)(2,1)S(1)} %reshape.630), channel_id=1, replica_groups=mesh['dp'=4,'kv_0'=4,'kv_1'=4,'tp'=2] {'tp'}, dimensions={0} | all-to-all | bytes 4096 | tf_op jit(solution)/shard_map/all_to_all | solution.py:79
  77.3 1.8 %all-gather.5 = bf16[2,64,9]{1,2,0:T(8,128)(2,1)S(1)} all-gather(bf16[1,64,9]{1,2,0:T(8,128)(2,1)S(1)} %maximum_bitcast_fusion.3), channel_id=1, replica_groups=mesh['dp'=4,'kv_0'=4,'kv_1'=4,'tp'=2] {'tp'}, dimensions={0}, use_global_device_ids=true | all-gather | bytes 3456 | tf_op jit(solution)/shard_map/all_gather | solution.py:19
  79.3 0.2 fusion.59
  79.5 0.2 fusion.57
  79.7 0.6 transpose.84
  80.3 3.5 %all-to-all-start.3 = ((f32[16,8,1]{1,2,0:T(1,128)}), f32[16,8,1]{1,2,0:T(1,128)S(1)}, u32[]{:S(2)}, u32[]{:S(2)}) async-start(f32[16,8,1]{1,2,0:T(1,128)} %transpose.84), calls=%async_computation.3 | async-start | bytes 16384 | tf_op jit(solution)/shard_map/all_to_all | solution.py:85
  83.9 0.2 reshape.571
  84.1 0.8 copy.191
  84.9 5.3 %all-to-all-done.3 = f32[16,8,1]{1,2,0:T(1,128)S(1)} async-done(((f32[16,8,1]{1,2,0:T(1,128)}), f32[16,8,1]{1,2,0:T(1,128)S(1)}, u32[]{:S(2)}, u32[]{:S(2)}) %all-to-all-start.3) | async-done | bytes 544 | tf_op jit(solution)/shard_map/all_to_all | solution.py:85
  90.3 3.5 %all-to-all-start.2 = ((f32[16,16,176]{2,1,0:T(8,128)}), f32[16,16,176]{2,1,0:T(8,128)S(1)}, u32[]{:S(2)}, u32[]{:S(2)}) async-start(f32[16,16,176]{2,1,0:T(8,128)} %bitcast.218), calls=%async_computation.2 | async-start | bytes 524288 | tf_op jit(solution)/shard_map/all_to_all | solution.py:85
  93.8 7.5 %all-to-all-done.2 = f32[16,16,176]{2,1,0:T(8,128)S(1)} async-done(((f32[16,16,176]{2,1,0:T(8,128)}), f32[16,16,176]{2,1,0:T(8,128)S(1)}, u32[]{:S(2)}, u32[]{:S(2)}) %all-to-all-start.2) | async-done | bytes 180256 | tf_op jit(solution)/shard_map/all_to_all | solution.py:85
  101.5 9.4 %all_to_all.32 = bf16[16,8,176]{2,1,0:T(8,128)(2,1)S(1)} all-to-all(bf16[16,8,176]{2,1,0:T(8,128)(2,1)S(1)} %broadcast_in_dim.5), channel_id=1, replica_groups=mesh['dp'=4,'kv_0'=4,'kv_1'=4,'tp'=2] {'kv_0','kv_1'}, dimensions={0} | all-to-all | bytes 90112 | tf_op jit(solution)/shard_map/all_to_all | solution.py:29
  110.9 0.1 reshape.572
  111.0 0.2 convolution_convert_fusion
  111.4 7.3 %all_to_all.33 = bf16[2,2,256]{2,1,0:T(2,128)(2,1)S(1)} all-to-all(bf16[2,2,256]{2,1,0:T(2,128)(2,1)S(1)} %reshape.632), channel_id=1, replica_groups=mesh['dp'=4,'kv_0'=4,'kv_1'=4,'tp'=2] {'tp'}, dimensions={0} | all-to-all | bytes 4096 | tf_op jit(solution)/shard_map/all_to_all | solution.py:79
  118.8 0.6 add_convert_fusion.2
  (92 shorter events, 3.3 us)
Async XLA Ops:
  0.0 79.3 %copy-start = (bf16[128,2816]{1,0:T(8,128)(2,1)S(1)}, bf16[128,2816]{1,0:T(8,128)(2,1)}, u32[]{:S(2)}) copy-start(bf16[128,2816]{1,0:T(8,128)(2,1)} %param.27) | copy-start | bytes 2162692
  10.1 21.5 %all-to-all-start = ((f32[16,1,12296]{2,1,0:T(1,128)}), f32[16,1,12296]{2,1,0:T(1,128)S(1)}, u32[]{:S(2)}, u32[]{:S(2)}) async-start(f32[16,1,12296]{2,1,0:T(1,128)} %broadcast_in_dim.4), calls=%async_computation | async-start | bytes 1589248 | tf_op jit(solution)/shard_map/all_to_all | solution.py:29
  39.1 27.2 %copy-start.4 = (f32[4]{0:T(128)S(1)}, f32[4]{0:T(128)}, u32[]{:S(2)}) copy-start(f32[4]{0:T(128)} %param.23) | copy-start | bytes 52
  39.1 27.5 %copy-start.6 = (bf16[512,128]{1,0:T(8,128)(2,1)S(1)}, bf16[512,128]{1,0:T(8,128)(2,1)}, u32[]{:S(2)}) copy-start(bf16[512,128]{1,0:T(8,128)(2,1)} %param.25) | copy-start | bytes 393220
  39.2 38.1 %copy-start.3 = (bf16[8,64]{1,0:T(8,128)(2,1)S(1)}, bf16[8,64]{1,0:T(8,128)(2,1)}, u32[]{:S(2)}) copy-start(bf16[8,64]{1,0:T(8,128)(2,1)} %param.16) | copy-start | bytes 3076
  39.2 38.1 %copy-start.5 = (bf16[64]{0:T(256)(128)(2,1)S(1)}, bf16[64]{0:T(256)(128)(2,1)}, u32[]{:S(2)}) copy-start(bf16[64]{0:T(256)(128)(2,1)} %param.26) | copy-start | bytes 388
  39.2 40.3 %copy-start.1 = (bf16[128,2816]{1,0:T(8,128)(2,1)S(1)}, bf16[128,2816]{1,0:T(8,128)(2,1)}, u32[]{:S(2)}) copy-start(bf16[128,2816]{1,0:T(8,128)(2,1)} %param.28) | copy-start | bytes 2162692
  39.2 71.8 %copy-start.2 = (bf16[2816,128]{1,0:T(8,128)(2,1)S(1)}, bf16[2816,128]{1,0:T(8,128)(2,1)}, u32[]{:S(2)}) copy-start(bf16[2816,128]{1,0:T(8,128)(2,1)} %param.29) | copy-start | bytes 2162692
  80.3 9.9 %all-to-all-start.3 = ((f32[16,8,1]{1,2,0:T(1,128)}), f32[16,8,1]{1,2,0:T(1,128)S(1)}, u32[]{:S(2)}, u32[]{:S(2)}) async-start(f32[16,8,1]{1,2,0:T(1,128)} %transpose.84), calls=%async_computation.3 | async-start | bytes 16384 | tf_op jit(solution)/shard_map/all_to_all | solution.py:85
  90.3 11.1 %all-to-all-start.2 = ((f32[16,16,176]{2,1,0:T(8,128)}), f32[16,16,176]{2,1,0:T(8,128)S(1)}, u32[]{:S(2)}, u32[]{:S(2)}) async-start(f32[16,16,176]{2,1,0:T(8,128)} %bitcast.218), calls=%async_computation.2 | async-start | bytes 524288 | tf_op jit(solution)/shard_map/all_to_all | solution.py:85
where the time goes:
time: 120 us; the launch traced here: 119 us
  blocking collectives  50.7 us (42%)
  waiting for transfers between devices  25.7 us (21%)
  matrix products  16.4 us (14%)
  starting transfers between devices  14.9 us (12%)
  local copies, waits for them, and re-layouts  7.53 us (6%)
  other arithmetic  3.79 us (3%)
    all_gather x2, blocking collectives, collected_together(): both, at, found = (lax.all_gather(jnp.concatenate(lines), axis), 0, {})  19.2 us
    all_to_all x2, blocking collectives, sent_and_summed(): lax.all_to_all(parts, axis, split_axis=0, concat_axis=0, tiled=True)  17.4 us
    all_to_all x1, waiting for transfers between devices, copy_for_each(): return lax.all_to_all(copies, axis, split_axis=0, concat_axis=0, tiled=True)  12.8 us
    all_to_all x2, waiting for transfers between devices, sent_and_summed_2(): lax.all_to_all(split_up(value, dim, devices), axis, 0, 0, tiled=True)  12.8 us
    all_to_all x1, blocking collectives, copy_for_each(): return lax.all_to_all(copies, axis, split_axis=0, concat_axis=0, tiled=True)  9.4 us
    all_to_all x1, starting transfers between devices, copy_for_each(): return lax.all_to_all(copies, axis, split_axis=0, concat_axis=0, tiled=True)  7.88 us
    all_to_all x2, starting transfers between devices, sent_and_summed_2(): lax.all_to_all(split_up(value, dim, devices), axis, 0, 0, tiled=True)  7.01 us
    dot_general x1, matrix products, shards(): jnp.einsum('bhmk,bphk->bhmp', padded_query_rows, key_cache, preferred_ele...  5.74 us
  transfers between devices with their start and end apart: 3, of which 3 were waited for; matrix products, arithmetic and copies ran while one was open for 2% of the time, Pallas kernels for 0%

commit v1 on v0

--- a/solution.py
+++ b/solution.py
@@ -16,7 +16,11 @@
 def turned_gather(arrays, axis, dims):
     turned = [jnp.moveaxis(a, dim, 0) for a, dim in zip(arrays, dims)]
     both = jnp.concatenate([t.reshape(len(t), -1) for t in turned], axis=1)
-    filled, at, done = (lax.all_gather(both, axis, axis=0, tiled=True), 0, [])
+    hold_teams = lambda local_values, peer_axis, axis_k: jnp.concatenate(
+        lax.all_to_all(jnp.stack([local_values] * lax.axis_size(peer_axis)), peer_axis, 0, 0),
+        axis=axis_k,
+    )
+    filled, at, done = (hold_teams(both, axis, 0), 0, [])
     for t, dim in zip(turned, dims):
         piece = filled[:, at : at + t[0].size].reshape(-1, *t.shape[1:])
         done.append(jnp.moveaxis(piece, 0, dim))

time: 120 us -> 124 us (1.033)
  blocking collectives: 50.7 us -> 54.4 us
    all_to_all x0 -> x2, blocking collectives: none -> 8.42 us  [turned_gather(): lax.all_to_all(jnp.stack([local_values] * lax.axis_size(peer_axis)), peer...]
    all_gather x2 -> x0, blocking collectives: 4.66 us -> none  [turned_gather(): filled, at, done = (lax.all_gather(both, axis, axis=0, tiled=True), 0, [])]
where the time goes in v1:
time: 124 us; the launch traced here: 123 us
  blocking collectives  54.4 us (44%)
  waiting for transfers between devices  25.7 us (21%)
  matrix products  16.4 us (13%)
  starting transfers between devices  14.9 us (12%)
  local copies, waits for them, and re-layouts  7.89 us (6%)
  other arithmetic  3.81 us (3%)
    all_gather x2, blocking collectives, collected_together(): both, at, found = (lax.all_gather(jnp.concatenate(lines), axis), 0, {})  19.2 us
    all_to_all x2, blocking collectives, sent_and_summed(): lax.all_to_all(parts, axis, split_axis=0, concat_axis=0, tiled=True)  17.4 us
    all_to_all x1, waiting for transfers between devices, copy_for_each(): return lax.all_to_all(copies, axis, split_axis=0, concat_axis=0, tiled=True)  12.9 us
    all_to_all x2, waiting for transfers between devices, sent_and_summed_2(): lax.all_to_all(split_up(value, dim, devices), axis, 0, 0, tiled=True)  12.8 us
    all_to_all x1, blocking collectives, copy_for_each(): return lax.all_to_all(copies, axis, split_axis=0, concat_axis=0, tiled=True)  9.39 us
    all_to_all x2, blocking collectives, turned_gather(): lax.all_to_all(jnp.stack([local_values] * lax.axis_size(peer_axis)), peer...  8.42 us
    all_to_all x1, starting transfers between devices, copy_for_each(): return lax.all_to_all(copies, axis, split_axis=0, concat_axis=0, tiled=True)  7.88 us
    all_to_all x2, starting transfers between devices, sent_and_summed_2(): lax.all_to_all(split_up(value, dim, devices), axis, 0, 0, tiled=True)  7.01 us
  transfers between devices with their start and end apart: 3, of which 3 were waited for; matrix products, arithmetic and copies ran while one was open for 2% of the time, Pallas kernels for 0%

profile of v1, /device:TPU:1, one launch (start us, length us, event | category | flops | bytes accessed | tf_op | source)
XLA Modules:
  0.0 123.5 jit_solution(14772903415737908162)
XLA Ops:
  0.0 0.8 maximum_bitcast_fusion.2
  0.9 4.7 %all_to_all.41 = bf16[2,2,288]{2,1,0:T(2,128)(2,1)S(1)} all-to-all(bf16[2,2,288]{2,1,0:T(2,128)(2,1)S(1)} %reshape.634), channel_id=1, replica_groups=mesh['dp'=4,'kv_0'=4,'kv_1'=4,'tp'=2] {'tp'}, dimensions={0} | all-to-all | bytes 4608 | tf_op jit(solution)/shard_map/all_to_all | solution.py:20
  5.9 1.0 convolution_bitcast_fusion.4
  6.9 1.0 convolution_bitcast_fusion.3
  7.9 1.0 convolution_bitcast_fusion.2
  8.9 1.0 convolution_bitcast_fusion.1
  9.8 1.0 convolution_bitcast_fusion
  10.9 1.3 %broadcast_in_dim.4 = f32[16,1,12296]{2,1,0:T(1,128)} broadcast(f32[12296]{0:T(1024)S(1)} %constant_dynamic-update-slice_fusion), dimensions={2} | broadcast | bytes 836128 | tf_op jit(solution)/shard_map/broadcast_in_dim | solution.py:32
  12.2 7.9 %all-to-all-start.1 = ((f32[16,1,12296]{2,1,0:T(1,128)}), f32[16,1,12296]{2,1,0:T(1,128)S(1)}, u32[]{:S(2)}, u32[]{:S(2)}) async-start(f32[16,1,12296]{2,1,0:T(1,128)} %broadcast_in_dim.4), calls=%async_computation.1 | async-start | bytes 1589248 | tf_op jit(solution)/shard_map/all_to_all | solution.py:33
  20.2 0.7 broadcast_bitcast_fusion
  20.9 12.9 %all-to-all-done.1 = f32[16,1,12296]{2,1,0:T(1,128)S(1)} async-done(((f32[16,1,12296]{2,1,0:T(1,128)}), f32[16,1,12296]{2,1,0:T(1,128)S(1)}, u32[]{:S(2)}, u32[]{:S(2)}) %all-to-all-start.1) | async-done | bytes 786976 | tf_op jit(solution)/shard_map/all_to_all | solution.py:33
  33.8 0.5 reduce_sum.91
  35.0 5.7 %fusion.94 = (f32[8,4,2]{2,1,0:T(4,128)S(1)}, f32[8,4,2,1024]{3,2,1,0:T(2,128)S(1)}) fusion(bf16[8,1024,4,128]{3,2,1,0:T(4,128)(2,1)} %param.30, bf16[8,4,1,128]{3,2,1,0:T(2,128)(2,1)S(1)} %copy.107, bf16[8,4,1,128]{3,2,1,0:T(2,128)(2,1)S(1)} %copy.106), kind=kOutput, calls=%fused_computation.186 | convolution fusion | flops 16940992 | bytes 8667392 | tf_op jit(solution)/shard_map/bhmk,bphk->bhmp/dot_general | solution.py:204
  40.8 0.1 reshape.563
  40.9 0.3 fusion.7
  41.3 4.9 %fusion = f32[8,4,2,128]{3,2,1,0:T(2,128)S(1)} fusion(bf16[8,1024,4,128]{3,2,1,0:T(4,128)(2,1)} %param.31, f32[8,4,2,1024]{3,2,1,0:T(2,128)S(1)} %get-tuple-element.57, f32[8,4,2]{2,1,0:T(4,128)S(1)} %get-tuple-element.56), kind=kOutput, calls=%fused_computation | convolution fusion | flops 16908288 | bytes 8683776 | tf_op jit(solution)/shard_map/bhmp,bphe->bhme/dot_general | solution.py:212
  46.4 9.5 %all-gather.2 = f32[4,66,128]{2,1,0:T(8,128)S(1)} all-gather(f32[1,66,128]{2,1,0:T(8,128)S(1)} %maximum_bitcast_fusion), channel_id=2, replica_groups=mesh['dp'=4,'kv_0'=4,'kv_1'=4,'tp'=2] {'kv_0'}, dimensions={0}, use_global_device_ids=true | all-gather | bytes 168960 | tf_op jit(solution)/shard_map/all_gather | solution.py:58
  56.1 9.6 %all-gather.3 = f32[4,66,128]{2,1,0:T(8,128)S(1)} all-gather(f32[1,66,128]{2,1,0:T(8,128)S(1)} %maximum_bitcast_fusion.1), channel_id=3, replica_groups=mesh['dp'=4,'kv_0'=4,'kv_1'=4,'tp'=2] {'kv_1'}, dimensions={0}, use_global_device_ids=true | all-gather | bytes 168960 | tf_op jit(solution)/shard_map/all_gather | solution.py:58
  65.9 0.1 copy.111
  66.2 0.1 copy.112
  66.3 0.1 squeeze.107
  66.4 0.1 copy.116
  66.7 0.1 copy.119
  67.0 0.1 copy.122
  67.1 0.1 squeeze.112
  67.2 0.1 copy.123
  67.5 0.1 copy.124
  67.8 0.1 copy.125
  68.0 0.2 multiply_reduce_fusion
  68.2 0.2 fusion.23
  68.4 0.2 fusion.38
  68.7 0.2 convolution_convert_fusion.1
  69.1 10.2 %all_to_all.42 = bf16[2,2,256]{2,1,0:T(2,128)(2,1)S(1)} all-to-all(bf16[2,2,256]{2,1,0:T(2,128)(2,1)S(1)} %reshape.636), channel_id=1, replica_groups=mesh['dp'=4,'kv_0'=4,'kv_1'=4,'tp'=2] {'tp'}, dimensions={0} | all-to-all | bytes 4096 | tf_op jit(solution)/shard_map/all_to_all | solution.py:83
  79.5 3.7 %all_to_all.43 = bf16[2,2,288]{2,1,0:T(2,128)(2,1)S(1)} all-to-all(bf16[2,2,288]{2,1,0:T(2,128)(2,1)S(1)} %reshape.638), channel_id=1, replica_groups=mesh['dp'=4,'kv_0'=4,'kv_1'=4,'tp'=2] {'tp'}, dimensions={0} | all-to-all | bytes 4608 | tf_op jit(solution)/shard_map/all_to_all | solution.py:20
  83.5 0.2 fusion.59
  83.7 0.2 fusion.57
  83.9 0.6 transpose.84
  84.5 3.5 %all-to-all-start.5 = ((f32[16,8,1]{1,2,0:T(1,128)}), f32[16,8,1]{1,2,0:T(1,128)S(1)}, u32[]{:S(2)}, u32[]{:S(2)}) async-start(f32[16,8,1]{1,2,0:T(1,128)} %transpose.84), calls=%async_computation.5 | async-start | bytes 16384 | tf_op jit(solution)/shard_map/all_to_all | solution.py:89
  88.0 0.2 reshape.579
  88.2 0.8 copy.191
  89.1 5.3 %all-to-all-done.5 = f32[16,8,1]{1,2,0:T(1,128)S(1)} async-done(((f32[16,8,1]{1,2,0:T(1,128)}), f32[16,8,1]{1,2,0:T(1,128)S(1)}, u32[]{:S(2)}, u32[]{:S(2)}) %all-to-all-start.5) | async-done | bytes 544 | tf_op jit(solution)/shard_map/all_to_all | solution.py:89
  94.4 3.5 %all-to-all-start.4 = ((f32[16,16,176]{2,1,0:T(8,128)}), f32[16,16,176]{2,1,0:T(8,128)S(1)}, u32[]{:S(2)}, u32[]{:S(2)}) async-start(f32[16,16,176]{2,1,0:T(8,128)} %bitcast.224), calls=%async_computation.4 | async-start | bytes 524288 | tf_op jit(solution)/shard_map/all_to_all | solution.py:89
  98.0 7.5 %all-to-all-done.4 = f32[16,16,176]{2,1,0:T(8,128)S(1)} async-done(((f32[16,16,176]{2,1,0:T(8,128)}), f32[16,16,176]{2,1,0:T(8,128)S(1)}, u32[]{:S(2)}, u32[]{:S(2)}) %all-to-all-start.4) | async-done | bytes 180256 | tf_op jit(solution)/shard_map/all_to_all | solution.py:89
  105.6 9.4 %all_to_all.44 = bf16[16,8,176]{2,1,0:T(8,128)(2,1)S(1)} all-to-all(bf16[16,8,176]{2,1,0:T(8,128)(2,1)S(1)} %broadcast_in_dim.5), channel_id=1, replica_groups=mesh['dp'=4,'kv_0'=4,'kv_1'=4,'tp'=2] {'kv_0','kv_1'}, dimensions={0} | all-to-all | bytes 90112 | tf_op jit(solution)/shard_map/all_to_all | solution.py:33
  115.0 0.1 reshape.580
  115.2 0.2 convolution_convert_fusion
  115.6 7.3 %all_to_all.45 = bf16[2,2,256]{2,1,0:T(2,128)(2,1)S(1)} all-to-all(bf16[2,2,256]{2,1,0:T(2,128)(2,1)S(1)} %reshape.640), channel_id=1, replica_groups=mesh['dp'=4,'kv_0'=4,'kv_1'=4,'tp'=2] {'tp'}, dimensions={0} | all-to-all | bytes 4096 | tf_op jit(solution)/shard_map/all_to_all | solution.py:83
  122.9 0.6 add_convert_fusion.2
  (98 shorter events, 3.7 us)
Async XLA Ops:
  0.0 83.5 %copy-start = (bf16[128,2816]{1,0:T(8,128)(2,1)S(1)}, bf16[128,2816]{1,0:T(8,128)(2,1)}, u32[]{:S(2)}) copy-start(bf16[128,2816]{1,0:T(8,128)(2,1)} %param.27) | copy-start | bytes 2162692
  12.2 21.5 %all-to-all-start.1 = ((f32[16,1,12296]{2,1,0:T(1,128)}), f32[16,1,12296]{2,1,0:T(1,128)S(1)}, u32[]{:S(2)}, u32[]{:S(2)}) async-start(f32[16,1,12296]{2,1,0:T(1,128)} %broadcast_in_dim.4), calls=%async_computation.1 | async-start | bytes 1589248 | tf_op jit(solution)/shard_map/all_to_all | solution.py:33
  41.2 27.2 %copy-start.4 = (f32[4]{0:T(128)S(1)}, f32[4]{0:T(128)}, u32[]{:S(2)}) copy-start(f32[4]{0:T(128)} %param.23) | copy-start | bytes 52
  41.2 27.5 %copy-start.6 = (bf16[512,128]{1,0:T(8,128)(2,1)S(1)}, bf16[512,128]{1,0:T(8,128)(2,1)}, u32[]{:S(2)}) copy-start(bf16[512,128]{1,0:T(8,128)(2,1)} %param.25) | copy-start | bytes 393220
  41.2 38.1 %copy-start.3 = (bf16[8,64]{1,0:T(8,128)(2,1)S(1)}, bf16[8,64]{1,0:T(8,128)(2,1)}, u32[]{:S(2)}) copy-start(bf16[8,64]{1,0:T(8,128)(2,1)} %param.16) | copy-start | bytes 3076
  41.3 38.1 %copy-start.5 = (bf16[64]{0:T(256)(128)(2,1)S(1)}, bf16[64]{0:T(256)(128)(2,1)}, u32[]{:S(2)}) copy-start(bf16[64]{0:T(256)(128)(2,1)} %param.26) | copy-start | bytes 388
  41.3 42.4 %copy-start.1 = (bf16[128,2816]{1,0:T(8,128)(2,1)S(1)}, bf16[128,2816]{1,0:T(8,128)(2,1)}, u32[]{:S(2)}) copy-start(bf16[128,2816]{1,0:T(8,128)(2,1)} %param.28) | copy-start | bytes 2162692
  41.3 73.9 %copy-start.2 = (bf16[2816,128]{1,0:T(8,128)(2,1)S(1)}, bf16[2816,128]{1,0:T(8,128)(2,1)}, u32[]{:S(2)}) copy-start(bf16[2816,128]{1,0:T(8,128)(2,1)} %param.29) | copy-start | bytes 2162692
  84.5 9.9 %all-to-all-start.5 = ((f32[16,8,1]{1,2,0:T(1,128)}), f32[16,8,1]{1,2,0:T(1,128)S(1)}, u32[]{:S(2)}, u32[]{:S(2)}) async-start(f32[16,8,1]{1,2,0:T(1,128)} %transpose.84), calls=%async_computation.5 | async-start | bytes 16384 | tf_op jit(solution)/shard_map/all_to_all | solution.py:89
  94.4 11.1 %all-to-all-start.4 = ((f32[16,16,176]{2,1,0:T(8,128)}), f32[16,16,176]{2,1,0:T(8,128)S(1)}, u32[]{:S(2)}, u32[]{:S(2)}) async-start(f32[16,16,176]{2,1,0:T(8,128)} %bitcast.224), calls=%async_computation.4 | async-start | bytes 524288 | tf_op jit(solution)/shard_map/all_to_all | solution.py:89
